TPU v7x, 32 devices: a whole 2x2x4 slice. The times are simulated.
32 devices in a mesh: sp: 16 (over z, y, core), tp: 2 (over x).
Axes of the slice: x: 2, y: 2, z: 4, core: 2. Of those that a mesh axis runs over, the one named last changes fastest.
Arguments:
- residual: bfloat16 [2048, 2048], P(('sp', 'tp')), may hold values from -6 to 6
- q_small: bfloat16 [2048, 1024], P('sp', 'tp'), may hold values from -6 to 6
- k_small: bfloat16 [2048, 1024], P('sp', 'tp'), may hold values from -6 to 6
- v_small: bfloat16 [2048, 1024], P('sp', 'tp'), may hold values from -6 to 6
- q_large: bfloat16 [2048, 1024], P('sp', 'tp'), may hold values from -6 to 6
- k_large: bfloat16 [2048, 1024], P('sp', 'tp'), may hold values from -6 to 6
- v_large: bfloat16 [2048, 1024], P('sp', 'tp'), may hold values from -6 to 6
- forget_small: float32 [2048, 16], P('sp', 'tp'), may hold values from 0 to 20
- forget_large: float32 [2048, 8], P('sp', 'tp'), may hold values from 0 to 20
- w_out_small: bfloat16 [1024, 2048], P('tp'), may hold values from -0.125 to 0.125
- w_out_large: bfloat16 [1024, 2048], P('tp'), may hold values from -0.125 to 0.125
- norm_gain: float32 [2048], replicated, may hold values from 0.1 to 1.9
- w_gate: bfloat16 [2048, 4096], P('sp', 'tp'), may hold values from -0.125 to 0.125
- w_up: bfloat16 [2048, 4096], P('sp', 'tp'), may hold values from -0.125 to 0.125
- conv_gate: float32 [3, 4096], P(None, 'tp'), may hold values from -3 to 3
- conv_up: float32 [3, 4096], P(None, 'tp'), may hold values from -3 to 3
- w_down: bfloat16 [4096, 2048], P('tp', 'sp'), may hold values from -0.09375 to 0.09375
Outputs:
- mixed: bfloat16 [2048, 2048], P(('sp', 'tp'))
All inputs are finite; a program needn't handle non-finite values.
Results may differ from a plain program's by a relative error of at most 0.015.
Values may be sent and summed in bfloat16 or wider, within the bound.
A program may use at most 64 MiB of HBM per device.

v0:
```python
import jax
import jax.numpy as jnp
from jax import lax
from jax.sharding import PartitionSpec as P

EPS = 1e-06
NEG = -1e30


def from_behind(block, axis, distance):
    devices = range(lax.axis_size(axis))
    route = [(i - distance, i) for i in devices if i - distance in devices]
    return lax.ppermute(block, axis, route)


def globalize(part, rows):
    heads = part.shape[1]
    blocks = part.reshape(-1, rows, heads)
    totals = blocks[:, -1, :]
    before = jnp.cumsum(totals, axis=0) - totals
    return (blocks + before[:, None, :]).reshape(part.shape)


def attend(carry, keys, values, queries, cum_own, cum_every, qpos):
    top, denom, accum = carry
    count = keys.shape[0]
    heads = queries.shape[1]
    size = queries.shape[2]
    keys = keys.reshape(count, heads, size)
    values = values.reshape(count, heads, size)
    kpos = jnp.arange(count, dtype=jnp.int32)
    scores = jnp.einsum(
        "qhd,khd->qhk", queries, keys, preferred_element_type=jnp.float32
    ) * size ** (-0.5)
    scores = scores + cum_own[:, :, None] - cum_every.T[None, :, :]
    keep = (kpos[None, :] <= qpos[:, None])[:, None, :]
    scores = jnp.where(keep, scores, NEG)
    new_top = jnp.maximum(top, jnp.max(scores, axis=-1))
    weights = jnp.where(keep, jnp.exp(scores - new_top[:, :, None]), 0.0)
    denom = jnp.sum(weights, axis=-1)
    accum = jnp.einsum(
        "qhk,khd->qhd", weights.astype(jnp.bfloat16), values, preferred_element_type=jnp.float32
    )
    return (new_top, denom, accum)


def finish(carry):
    top, denom, accum = carry
    attended = accum / denom[:, :, None]
    normed = attended * lax.rsqrt(jnp.mean(attended * attended, axis=-1, keepdims=True) + EPS)
    return normed.astype(jnp.bfloat16).reshape(attended.shape[0], -1)


def empty_carry(rows, heads, size):
    return (
        jnp.full((rows, heads), NEG, jnp.float32),
        jnp.zeros((rows, heads), jnp.float32),
        jnp.zeros((rows, heads, size), jnp.float32),
    )


def body(
    residual,
    q_small,
    k_small,
    v_small,
    q_large,
    k_large,
    v_large,
    forget_small,
    forget_large,
    w_out_small,
    w_out_large,
    norm_gain,
    w_gate,
    w_up,
    conv_gate,
    conv_up,
    w_down,
):
    rows = q_small.shape[0]
    offset = lax.axis_index("sp") * rows
    qpos = offset + jnp.arange(rows, dtype=jnp.int32)
    gathered = (
        lax.all_gather(w_gate, "sp", axis=0, tiled=True),
        lax.all_gather(w_up, "sp", axis=0, tiled=True),
        lax.all_gather(w_down, "sp", axis=1, tiled=True),
    )
    local_small = jnp.cumsum(jax.nn.log_sigmoid(forget_small), axis=0)
    local_large = jnp.cumsum(jax.nn.log_sigmoid(forget_large), axis=0)
    part_small, part_large = (
        lax.all_gather(local_small, "sp", axis=0, tiled=True),
        lax.all_gather(local_large, "sp", axis=0, tiled=True),
    )
    every_small = globalize(part_small, rows)
    every_large = globalize(part_large, rows)
    cum_small = lax.dynamic_slice_in_dim(every_small, offset, rows, 0)
    cum_large = lax.dynamic_slice_in_dim(every_large, offset, rows, 0)
    heads_small = forget_small.shape[1]
    heads_large = forget_large.shape[1]
    queries_small = q_small.reshape(rows, heads_small, -1)
    queries_large = q_large.reshape(rows, heads_large, -1)
    start_carry = (
        empty_carry(rows, heads_small, queries_small.shape[2]),
        empty_carry(rows, heads_large, queries_large.shape[2]),
    )
    keys_s = lax.all_gather(k_small, "sp", axis=0, tiled=True)
    values_s = lax.all_gather(v_small, "sp", axis=0, tiled=True)
    keys_l = lax.all_gather(k_large, "sp", axis=0, tiled=True)
    values_l = lax.all_gather(v_large, "sp", axis=0, tiled=True)
    small = attend(start_carry[0], keys_s, values_s, queries_small, cum_small, every_small, qpos)
    large = attend(start_carry[1], keys_l, values_l, queries_large, cum_large, every_large, qpos)
    normed_small = finish(small)
    normed_large = finish(large)
    first_part = jnp.dot(normed_small, w_out_small, preferred_element_type=jnp.float32)
    projected = lax.psum_scatter(
        (
            first_part + jnp.dot(normed_large, w_out_large, preferred_element_type=jnp.float32)
        ).astype(jnp.bfloat16),
        "tp",
        scatter_dimension=0,
        tiled=True,
    ).astype(jnp.float32)
    first = residual.astype(jnp.float32) + projected
    normal = (
        first * lax.rsqrt(jnp.mean(first * first, axis=-1, keepdims=True) + EPS) * norm_gain
    ).astype(jnp.bfloat16)
    gate_full, up_full, down_full = gathered
    piece = lax.all_gather(normal, "tp", axis=0, tiled=True)
    gate_part = jnp.dot(piece, gate_full, preferred_element_type=jnp.float32).astype(jnp.bfloat16)
    up_part = jnp.dot(piece, up_full, preferred_element_type=jnp.float32).astype(jnp.bfloat16)
    both = jnp.concatenate([gate_part, up_part], axis=1)
    width = both.shape[0]
    rim = from_behind(both[width - 2 :], "sp", 1)
    extended = jnp.concatenate([rim, both], axis=0).astype(jnp.float32)
    taps = jnp.concatenate([conv_gate, conv_up], axis=1)
    conv = (
        taps[0] * extended[0:width]
        + taps[1] * extended[1 : width + 1]
        + taps[2] * extended[2 : width + 2]
    )
    half = gate_full.shape[1]
    hidden = (jax.nn.silu(conv[:, :half]) * conv[:, half:]).astype(jnp.bfloat16)
    mixed = first + lax.psum_scatter(
        jnp.dot(hidden, down_full, preferred_element_type=jnp.float32).astype(jnp.bfloat16),
        "tp",
        scatter_dimension=0,
        tiled=True,
    ).astype(jnp.float32)
    return mixed.astype(jnp.bfloat16)


def solution(mesh):
    placed = (
        P(("sp", "tp"), None),
        P("sp", "tp"),
        P("sp", "tp"),
        P("sp", "tp"),
        P("sp", "tp"),
        P("sp", "tp"),
        P("sp", "tp"),
        P("sp", "tp"),
        P("sp", "tp"),
        P("tp", None),
        P("tp", None),
        P(),
        P("sp", "tp"),
        P("sp", "tp"),
        P(None, "tp"),
        P(None, "tp"),
        P("tp", "sp"),
    )
    return jax.shard_map(
        body, mesh=mesh, in_specs=placed, out_specs=P(("sp", "tp"), None), check_vma=False
    )
```

profile of v0, /device:TPU:0, one launch (start us, length us, event | category | flops | bytes accessed | tf_op | source)
XLA Modules:
  0.0 472.0 jit_solution(16428870450614130786)
XLA Ops:
  8.1 1.7 copy.44
  11.4 27.1 %all_gather.34 = f32[2048,4]{1,0:T(8,128)S(1)} all-gather(f32[128,4]{1,0:T(8,128)S(1)} %reduce_window_sum.46), channel_id=1, replica_groups=mesh['sp'=16,'tp'=2] {'sp'}, dimensions={0}, use_global_device_ids=true | all-gather | bytes 34816 | tf_op jit(solution)/shard_map/all_gather | solution.py:93
  38.8 24.5 %all_gather.31 = f32[2048,8]{1,0:T(8,128)S(1)} all-gather(f32[128,8]{1,0:T(8,128)S(1)} %reduce_window_sum.44), channel_id=1, replica_groups=mesh['sp'=16,'tp'=2] {'sp'}, dimensions={0}, use_global_device_ids=true | all-gather | bytes 69632 | tf_op jit(solution)/shard_map/all_gather | solution.py:92
  63.4 1.1 bitcast_add_fusion.3
  65.7 1.6 copy.41
  67.7 4.0 copy.52
  71.7 31.4 %all-gather.8.cloned.1.call-done = bf16[2048,512]{1,0:T(8,128)(2,1)} async-done(((bf16[128,512]{1,0:T(8,128)(2,1)}), bf16[2048,512]{1,0:T(8,128)(2,1)}) %all-gather.8.cloned.1.call-update) | async-done | bytes 2097168 | tf_op jit(solution)/shard_map/all_gather | solution.py:107
  103.0 4.0 copy.35
  107.0 38.0 %all-gather.12.cloned.1.call-done = bf16[2048,512]{0,1:T(8,128)(2,1)} async-done(((bf16[128,512]{0,1:T(8,128)(2,1)}), bf16[2048,512]{0,1:T(8,128)(2,1)}) %all-gather.12.cloned.1.call-update) | async-done | bytes 2097168 | tf_op jit(solution)/shard_map/all_gather | solution.py:109
  145.0 3.7 fusion.47
  150.3 1.2 multiply_reduce_fusion.1
  151.9 3.4 fusion.4
  155.3 3.2 copy-done.2
  158.5 3.1 fusion.2
  161.6 26.0 %all-gather.10.cloned.1.call-done = bf16[2048,512]{1,0:T(8,128)(2,1)} async-done(((bf16[128,512]{1,0:T(8,128)(2,1)}), bf16[2048,512]{1,0:T(8,128)(2,1)}) %all-gather.10.cloned.1.call-update) | async-done | bytes 2097168 | tf_op jit(solution)/shard_map/all_gather | solution.py:108
  187.6 3.9 copy.42
  191.5 6.6 %multiply_reduce_fusion.2 = (f32[128,8]{0,1:T(8,128)S(1)}, f32[128,8,64]{0,2,1:T(8,128)S(1)}) fusion(f32[128,8]{0,1:T(8,128)S(1)} %fusion.2, bf16[2048,8,64]{0,2,1:T(8,128)(2,1)} %bitcast.82, f32[8,2048,128]{2,1,0:T(8,128)} %copy-done.2, f32[128,8]{0,1:T(8,128)S(1)} %broadcast_maximum_fusion, f32[8,2048]{1,0:T(8,128)S(1)} %copy.41, f32[128,8]{0,1:T(8,128)S(1)} %copy.40, ...), kind=kOutput, calls=%fused_computation.49 | convolution fusion | flops 283311104 | bytes 11091968 | tf_op jit(solution)/shard_map/qhk,khd->qhd/dot_general | solution.py:41
  199.7 1.3 fusion.12
  203.2 11.3 %reduce-scatter.3.cloned.1.call-done = bf16[64,2048]{1,0:T(8,128)(2,1)} async-done(((bf16[128,2048]{1,0:T(8,128)(2,1)}), bf16[64,2048]{1,0:T(8,128)(2,1)}) %reduce-scatter.3.cloned.1.call-update) | async-done | bytes 262160 | tf_op jit(solution)/shard_map/reduce_scatter | solution.py:116
  214.6 1.1 multiply_reduce_fusion
  215.7 1.1 multiply_convert_fusion
  216.8 8.7 %all_gather.36 = bf16[128,2048]{1,0:T(8,128)(2,1)S(1)} all-gather(bf16[64,2048]{1,0:T(8,128)(2,1)S(1)} %multiply_convert_fusion), channel_id=1, replica_groups=mesh['sp'=16,'tp'=2] {'tp'}, dimensions={0}, use_global_device_ids=true | all-gather | bytes 786432 | tf_op jit(solution)/shard_map/all_gather | solution.py:129
  225.5 65.4 %all-gather.18.cloned.1.call-done = bf16[2048,2048]{1,0:T(8,128)(2,1)} async-done(((bf16[128,2048]{1,0:T(8,128)(2,1)}), bf16[2048,2048]{1,0:T(8,128)(2,1)}) %all-gather.18.cloned.1.call-update) | async-done | bytes 8388624 | tf_op jit(solution)/shard_map/all_gather | solution.py:86
  290.9 4.6 convolution_convert_fusion.1
  295.6 70.4 %all-gather.16.cloned.1.call-done = bf16[2048,2048]{1,0:T(8,128)(2,1)} async-done(((bf16[128,2048]{1,0:T(8,128)(2,1)}), bf16[2048,2048]{1,0:T(8,128)(2,1)}) %all-gather.16.cloned.1.call-update) | async-done | bytes 8388624 | tf_op jit(solution)/shard_map/all_gather | solution.py:85
  366.0 4.6 convolution_convert_fusion.2
  370.7 2.2 collective-permute-start
  373.9 2.0 fusion.15
  375.9 68.5 %all-gather.20.cloned.1.call-done = bf16[2048,2048]{1,0:T(8,128)(2,1)} async-done(((bf16[2048,128]{1,0:T(8,128)(2,1)}), bf16[2048,2048]{1,0:T(8,128)(2,1)}) %all-gather.20.cloned.1.call-update) | async-done | bytes 8388624 | tf_op jit(solution)/shard_map/all_gather | solution.py:87
  444.5 6.3 %convolution_convert_fusion = bf16[128,2048]{1,0:T(8,128)(2,1)} fusion(bf16[2048,2048]{1,0:T(8,128)(2,1)} %all-gather.20.cloned.1.call-done, f32[128,4096]{1,0:T(8,128)} %fusion.15), kind=kOutput, calls=%fused_computation.16 | convolution fusion | flops 1075576832 | bytes 11010048 | tf_op jit(solution)/shard_map/dot_general | solution.py:145
  450.8 13.0 %reduce-scatter.5.cloned.1.call-done = bf16[64,2048]{1,0:T(8,128)(2,1)} async-done(((bf16[128,2048]{1,0:T(8,128)(2,1)}), bf16[64,2048]{1,0:T(8,128)(2,1)}) %reduce-scatter.5.cloned.1.call-update) | async-done | bytes 262160 | tf_op jit(solution)/shard_map/reduce_scatter | solution.py:144
  463.8 1.7 add_convert_fusion
  (78 shorter events, 12.0 us)
Async XLA Ops:
  6.5 191.7 %copy-start = (bf16[512,2048]{1,0:T(8,128)(2,1)S(1)}, bf16[512,2048]{1,0:T(8,128)(2,1)}, u32[]{:S(2)}) copy-start(bf16[512,2048]{1,0:T(8,128)(2,1)} %param.26) | copy-start | bytes 6291460
  6.5 32.0 %copy-start.12 = (f32[128,8]{0,1:T(8,128)S(1)}, f32[128,8]{0,1:T(8,128)}, u32[]{:S(2)}) copy-start(f32[128,8]{0,1:T(8,128)} %param.24) | copy-start | bytes 12292
  6.5 61.1 %all-gather.14.cloned.1.call-start = ((), (), s32[]{:S(2)}) async-start(), calls=%async_computation.5 | async-start | bytes 2228224 | tf_op jit(solution)/shard_map/all_gather | solution.py:110
  7.3 95.8 %all-gather.8.cloned.1.call-start = ((), (), s32[]{:S(2)}) async-start(), calls=%async_computation.2 | async-start | bytes 2228224 | tf_op jit(solution)/shard_map/all_gather | solution.py:107
  8.0 137.0 %all-gather.12.cloned.1.call-start = ((), (), s32[]{:S(2)}) async-start(), calls=%async_computation.4 | async-start | bytes 2228224 | tf_op jit(solution)/shard_map/all_gather | solution.py:109
  9.7 177.8 %all-gather.10.cloned.1.call-start = ((), (), s32[]{:S(2)}) async-start(), calls=%async_computation.3 | async-start | bytes 2228224 | tf_op jit(solution)/shard_map/all_gather | solution.py:108
  10.3 204.2 %reduce-scatter.3.cloned.1.call-start = ((), (), s32[]{:S(2)}) async-start(), calls=%async_computation.6 | async-start | bytes 786432 | tf_op jit(solution)/shard_map/reduce_scatter | solution.py:116
  38.4 28.9 %copy-start.8 = (bf16[128,512]{1,0:T(8,128)(2,1)S(1)}, bf16[128,512]{1,0:T(8,128)(2,1)}, u32[]{:S(2)}) copy-start(bf16[128,512]{1,0:T(8,128)(2,1)} %param.18) | copy-start | bytes 393220
  67.6 77.4 %copy-start.13 = (bf16[128,512]{1,0:T(8,128)(2,1)S(1)}, bf16[128,512]{1,0:T(8,128)(2,1)}, u32[]{:S(2)}) copy-start(bf16[128,512]{1,0:T(8,128)(2,1)} %param.21) | copy-start | bytes 393220
  148.7 1.6 copy-start.7
  150.3 1.6 copy-start.6
  155.2 3.2 copy-start.2
  198.1 1.6 copy-start.5
  198.2 5.0 %copy-start.9 = (f32[3,2048]{1,0:T(4,128)S(1)}, f32[3,2048]{1,0:T(4,128)}, u32[]{:S(2)}) copy-start(f32[3,2048]{1,0:T(4,128)} %param.31) | copy-start | bytes 73732
  198.2 5.0 %copy-start.10 = (f32[3,2048]{1,0:T(4,128)S(1)}, f32[3,2048]{1,0:T(4,128)}, u32[]{:S(2)}) copy-start(f32[3,2048]{1,0:T(4,128)} %param.32) | copy-start | bytes 73732
  198.3 16.3 %copy-start.3 = (bf16[64,2048]{1,0:T(8,128)(2,1)S(1)}, bf16[64,2048]{1,0:T(8,128)(2,1)}, u32[]{:S(2)}) copy-start(bf16[64,2048]{1,0:T(8,128)(2,1)} %param.17) | copy-start | bytes 786436
  198.3 17.5 %copy-start.11 = (f32[2048]{0:T(1024)S(1)}, f32[2048]{0:T(1024)}, u32[]{:S(2)}) copy-start(f32[2048]{0:T(1024)} %param.28) | copy-start | bytes 24580
  201.1 89.8 %all-gather.18.cloned.1.call-start = ((), (), s32[]{:S(2)}) async-start(), calls=%async_computation.8 | async-start | bytes 8912896 | tf_op jit(solution)/shard_map/all_gather | solution.py:86
  201.6 164.3 %all-gather.16.cloned.1.call-start = ((), (), s32[]{:S(2)}) async-start(), calls=%async_computation.7 | async-start | bytes 8912896 | tf_op jit(solution)/shard_map/all_gather | solution.py:85
  202.4 242.1 %all-gather.20.cloned.1.call-start = ((), (), s32[]{:S(2)}) async-start(), calls=%async_computation.9 | async-start | bytes 8912896 | tf_op jit(solution)/shard_map/all_gather | solution.py:87
  203.1 260.6 %reduce-scatter.5.cloned.1.call-start = ((), (), s32[]{:S(2)}) async-start(), calls=%async_computation.10 | async-start | bytes 786432 | tf_op jit(solution)/shard_map/reduce_scatter | solution.py:144
  370.7 3.0 collective-permute-start
  375.9 87.8 %copy-start.4 = (bf16[64,2048]{1,0:T(8,128)(2,1)S(1)}, bf16[64,2048]{1,0:T(8,128)(2,1)}, u32[]{:S(2)}) copy-start(bf16[64,2048]{1,0:T(8,128)(2,1)} %reduce-scatter.3.cloned.1.call-done) | copy-start | bytes 786436
  444.5 21.0 %copy-start.1 = (bf16[512,2048]{1,0:T(8,128)(2,1)S(1)}, bf16[512,2048]{1,0:T(8,128)(2,1)}, u32[]{:S(2)}) copy-start(bf16[512,2048]{1,0:T(8,128)(2,1)} %param.26) | copy-start | bytes 6291460
Sparse Core Ops, SparseCore 0:
  9.5 49.7 all-gather.13
  61.4 41.5 all-gather.7
  105.2 39.7 all-gather.11
  147.0 40.5 all-gather.9
  201.2 13.3 reduce-scatter.2
  216.6 74.2 all-gather.17
  293.1 72.8 all-gather.15
  368.1 76.2 all-gather.19
  450.9 12.7 reduce-scatter.4
where the time goes:
time: 473 us; the launch traced here: 472 us
  waiting for transfers between devices  329 us (70%)
  blocking collectives  60.3 us (13%)
  matrix products  32.2 us (7%)
  local copies, waits for them, and re-layouts  22.4 us (5%)
  between operations  13.5 us (3%)
  other arithmetic  12.6 us (3%)
    all_gather x1, waiting for transfers between devices, body(): lax.all_gather(w_gate, 'sp', axis=0, tiled=True)  70.4 us
    all_gather x1, waiting for transfers between devices, body(): lax.all_gather(w_down, 'sp', axis=1, tiled=True)  68.5 us
    all_gather x1, waiting for transfers between devices, body(): lax.all_gather(w_up, 'sp', axis=0, tiled=True)  65.4 us
    all_gather x1, waiting for transfers between devices, body(): keys_l = lax.all_gather(k_large, 'sp', axis=0, tiled=True)  38 us
    all_gather x1, waiting for transfers between devices, body(): keys_s = lax.all_gather(k_small, 'sp', axis=0, tiled=True)  31.4 us
    all_gather x1, blocking collectives, body(): lax.all_gather(local_large, 'sp', axis=0, tiled=True)  27.1 us
    all_gather x1, waiting for transfers between devices, body(): values_s = lax.all_gather(v_small, 'sp', axis=0, tiled=True)  26 us
    all_gather x1, blocking collectives, body(): lax.all_gather(local_small, 'sp', axis=0, tiled=True)  24.5 us
  transfers between devices with their start and end apart: 10, of which 9 were waited for; matrix products, arithmetic and copies ran while one was open for 9% of the time, Pallas kernels for 0%

commit v1 on v0

--- a/solution.py
+++ b/solution.py
@@ -104,8 +104,16 @@
         empty_carry(rows, heads_small, queries_small.shape[2]),
         empty_carry(rows, heads_large, queries_large.shape[2]),
     )
-    keys_s = lax.all_gather(k_small, "sp", axis=0, tiled=True)
-    values_s = lax.all_gather(v_small, "sp", axis=0, tiled=True)
+
+    def _follow_threads(frame, matrix):
+        finding = jnp.split(
+            lax.all_gather(jnp.concatenate([frame, matrix], 1), "sp", axis=0, tiled=True),
+            [frame.shape[1]],
+            1,
+        )
+        return finding
+
+    keys_s, values_s = _follow_threads(k_small, v_small)
     keys_l = lax.all_gather(k_large, "sp", axis=0, tiled=True)
     values_l = lax.all_gather(v_large, "sp", axis=0, tiled=True)
     small = attend(start_carry[0], keys_s, values_s, queries_small, cum_small, every_small, qpos)

time: 473 us -> 459 us (0.970)
  waiting for transfers between devices: 329 us -> 311 us
    split x0 -> x3, local copies, waits for them, and re-layouts: none -> 12.5 us  [_follow_threads(): jnp.split(lax.all_gather(jnp.concatenate([frame, matrix], 1), 'sp', axis=...]
    all_gather x2 -> x1, waiting for transfers between devices: 57.4 us -> 45.2 us  [_follow_threads(): lax.all_gather(jnp.concatenate([frame, matrix], 1), 'sp', axis=0, tiled=T...]
    all_gather x2 -> x0, local copies, waits for them, and re-layouts: 7.94 us -> none  [the longest x1 4 us: body(): keys_s = lax.all_gather(k_small, 'sp', axis=0, tiled=True)]
  transfers between devices with their start and end apart: 10 -> 9, of which waited for: 9 -> 8; matrix products, arithmetic and copies ran while one was open for 9% -> 6% of each run, Pallas kernels for 0% -> 0%
where the time goes in v1:
time: 459 us; the launch traced here: 458 us
  waiting for transfers between devices  311 us (68%)
  blocking collectives  59.4 us (13%)
  matrix products  33.7 us (7%)
  local copies, waits for them, and re-layouts  21.2 us (5%)
  other arithmetic  16.8 us (4%)
  between operations  13.8 us (3%)
    all_gather x1, waiting for transfers between devices, body(): lax.all_gather(w_gate, 'sp', axis=0, tiled=True)  70.3 us
    all_gather x1, waiting for transfers between devices, body(): lax.all_gather(w_down, 'sp', axis=1, tiled=True)  68.5 us
    all_gather x1, waiting for transfers between devices, body(): lax.all_gather(w_up, 'sp', axis=0, tiled=True)  65.4 us
    all_gather x1, waiting for transfers between devices, _follow_threads(): lax.all_gather(jnp.concatenate([frame, matrix], 1), 'sp', axis=0, tiled=T...  45.2 us
    all_gather x1, waiting for transfers between devices, body(): keys_l = lax.all_gather(k_large, 'sp', axis=0, tiled=True)  33.9 us
    all_gather x1, blocking collectives, body(): lax.all_gather(local_large, 'sp', axis=0, tiled=True)  26.7 us
    all_gather x1, blocking collectives, body(): lax.all_gather(local_small, 'sp', axis=0, tiled=True)  24 us
    reduce_scatter x1, waiting for transfers between devices, body(): lax.psum_scatter(jnp.dot(hidden, down_full, preferred_element_type=jnp.fl...  13 us
  transfers between devices with their start and end apart: 9, of which 8 were waited for; matrix products, arithmetic and copies ran while one was open for 6% of the time, Pallas kernels for 0%

profile of v1, /device:TPU:0, one launch (start us, length us, event | category | flops | bytes accessed | tf_op | source)
XLA Modules:
  0.0 458.2 jit_solution(5734372286156607428)
XLA Ops:
  7.3 1.7 copy.44
  9.0 1.7 pad_maximum_fusion
  11.8 26.7 %all_gather.30 = f32[2048,4]{1,0:T(8,128)S(1)} all-gather(f32[128,4]{1,0:T(8,128)S(1)} %reduce_window_sum.46), channel_id=1, replica_groups=mesh['sp'=16,'tp'=2] {'sp'}, dimensions={0}, use_global_device_ids=true | all-gather | bytes 34816 | tf_op jit(solution)/shard_map/all_gather | solution.py:93
  39.4 24.0 %all_gather.28 = f32[2048,8]{1,0:T(8,128)S(1)} all-gather(f32[128,8]{1,0:T(8,128)S(1)} %reduce_window_sum.44), channel_id=1, replica_groups=mesh['sp'=16,'tp'=2] {'sp'}, dimensions={0}, use_global_device_ids=true | all-gather | bytes 69632 | tf_op jit(solution)/shard_map/all_gather | solution.py:92
  64.2 4.0 copy.52
  68.2 33.9 %all-gather.9.cloned.1.call-done = bf16[2048,512]{0,1:T(8,128)(2,1)} async-done(((bf16[128,512]{0,1:T(8,128)(2,1)}), bf16[2048,512]{0,1:T(8,128)(2,1)}) %all-gather.9.cloned.1.call-update) | async-done | bytes 2097168 | tf_op jit(solution)/shard_map/all_gather | solution.py:117
  102.1 3.7 fusion.48
  106.5 0.8 copy-done.6
  107.3 1.2 multiply_reduce_fusion.1
  108.6 45.2 %all-gather.7.cloned.1.call-done = bf16[2048,1024]{1,0:T(8,128)(2,1)} async-done(((bf16[128,1024]{1,0:T(8,128)(2,1)}), bf16[2048,1024]{1,0:T(8,128)(2,1)}) %all-gather.7.cloned.1.call-update) | async-done | bytes 4194320 | tf_op jit(solution)/shard_map/all_gather | solution.py:110
  153.7 4.6 fusion.46
  158.3 3.9 copy.36
  162.2 6.7 %fusion.4 = (f32[128,8]{0,1:T(8,128)S(1)}, f32[8,2048,128]{2,1,0:T(8,128)}) fusion(f32[8,2048]{1,0:T(8,128)S(1)} %copy.42, f32[128,8]{0,1:T(8,128)S(1)} %copy.41, pred[128,2048]{0,1:T(8,128)(4,1)S(1)} %iota_compare_fusion, bf16[2048,8,64]{0,2,1:T(8,128)(2,1)} %bitcast.82, bf16[128,8,64]{0,2,1:T(8,128)(2,1)S(1)} %bitcast.85), kind=kOutput, calls=%fused_computation.6 | convolution fusion | flops 278920192 | bytes 10952704 | tf_op jit(solution)/shard_map/qhd,khd->qhk/dot_general | solution.py:32
  168.9 3.9 copy.35
  172.8 6.6 %fusion.2 = f32[128,8]{0,1:T(8,128)S(1)} fusion(f32[8,2048,128]{2,1,0:T(8,128)} %get-tuple-element.11, f32[128,8]{0,1:T(8,128)S(1)} %broadcast_maximum_fusion, f32[8,2048]{1,0:T(8,128)S(1)} %copy.42, f32[128,8]{0,1:T(8,128)S(1)} %copy.41, pred[128,2048]{0,1:T(8,128)(4,1)S(1)} %iota_compare_fusion), kind=kLoop, calls=%fused_computation.4 | loop fusion | flops 14679040 | bytes 8728576 | tf_op jit(solution)/shard_map/reduce_sum | solution.py:40
  179.5 4.8 %multiply_reduce_fusion.2 = (f32[128,8]{0,1:T(8,128)S(1)}, f32[128,8,64]{0,2,1:T(8,128)S(1)}) fusion(f32[128,8]{0,1:T(8,128)S(1)} %fusion.2, bf16[2048,8,64]{0,2,1:T(8,128)(2,1)} %bitcast.81, f32[8,2048,128]{2,1,0:T(8,128)S(1)} %copy-done.2, f32[128,8]{0,1:T(8,128)S(1)} %broadcast_maximum_fusion, f32[8,2048]{1,0:T(8,128)S(1)} %copy.42, ...), kind=kOutput, calls=%fused_computation.50 | convolution fusion | flops 283311104 | bytes 11091968 | tf_op jit(solution)/shard_map/qhk,khd->qhd/dot_general | solution.py:41
  184.9 1.0 copy-done.5
  185.9 1.3 fusion.12
  189.3 11.3 %reduce-scatter.3.cloned.1.call-done = bf16[64,2048]{1,0:T(8,128)(2,1)} async-done(((bf16[128,2048]{1,0:T(8,128)(2,1)}), bf16[64,2048]{1,0:T(8,128)(2,1)}) %reduce-scatter.3.cloned.1.call-update) | async-done | bytes 262160 | tf_op jit(solution)/shard_map/reduce_scatter | solution.py:124
  200.6 1.1 multiply_reduce_fusion
  201.8 1.1 multiply_convert_fusion
  202.8 8.7 %all_gather.32 = bf16[128,2048]{1,0:T(8,128)(2,1)S(1)} all-gather(bf16[64,2048]{1,0:T(8,128)(2,1)S(1)} %multiply_convert_fusion), channel_id=1, replica_groups=mesh['sp'=16,'tp'=2] {'tp'}, dimensions={0}, use_global_device_ids=true | all-gather | bytes 786432 | tf_op jit(solution)/shard_map/all_gather | solution.py:137
  211.5 65.4 %all-gather.15.cloned.1.call-done = bf16[2048,2048]{1,0:T(8,128)(2,1)} async-done(((bf16[128,2048]{1,0:T(8,128)(2,1)}), bf16[2048,2048]{1,0:T(8,128)(2,1)}) %all-gather.15.cloned.1.call-update) | async-done | bytes 8388624 | tf_op jit(solution)/shard_map/all_gather | solution.py:86
  276.9 4.6 %convolution_convert_fusion.1 = bf16[128,2048]{1,0:T(8,128)(2,1)S(1)} fusion(bf16[128,2048]{1,0:T(8,128)(2,1)S(1)} %all_gather.32, bf16[2048,2048]{1,0:T(8,128)(2,1)} %all-gather.15.cloned.1.call-done), kind=kOutput, calls=%fused_computation.17 | convolution fusion | flops 1074003968 | bytes 9437184 | tf_op jit(solution)/shard_map/dot_general | solution.py:139
  281.6 70.3 %all-gather.13.cloned.1.call-done = bf16[2048,2048]{1,0:T(8,128)(2,1)} async-done(((bf16[128,2048]{1,0:T(8,128)(2,1)}), bf16[2048,2048]{1,0:T(8,128)(2,1)}) %all-gather.13.cloned.1.call-update) | async-done | bytes 8388624 | tf_op jit(solution)/shard_map/all_gather | solution.py:85
  351.9 4.6 %convolution_convert_fusion.2 = bf16[128,2048]{1,0:T(8,128)(2,1)S(1)} fusion(bf16[128,2048]{1,0:T(8,128)(2,1)S(1)} %all_gather.32, bf16[2048,2048]{1,0:T(8,128)(2,1)} %all-gather.13.cloned.1.call-done), kind=kOutput, calls=%fused_computation.18 | convolution fusion | flops 1074003968 | bytes 9437184 | tf_op jit(solution)/shard_map/dot_general | solution.py:138
  356.5 2.2 collective-permute-start
  359.8 2.0 fusion.15
  361.8 68.5 %all-gather.17.cloned.1.call-done = bf16[2048,2048]{1,0:T(8,128)(2,1)} async-done(((bf16[2048,128]{1,0:T(8,128)(2,1)}), bf16[2048,2048]{1,0:T(8,128)(2,1)}) %all-gather.17.cloned.1.call-update) | async-done | bytes 8388624 | tf_op jit(solution)/shard_map/all_gather | solution.py:87
  430.3 6.3 %convolution_convert_fusion = bf16[128,2048]{1,0:T(8,128)(2,1)} fusion(bf16[2048,2048]{1,0:T(8,128)(2,1)} %all-gather.17.cloned.1.call-done, f32[128,4096]{1,0:T(8,128)} %fusion.15), kind=kOutput, calls=%fused_computation.16 | convolution fusion | flops 1075576832 | bytes 11010048 | tf_op jit(solution)/shard_map/dot_general | solution.py:153
  436.7 13.0 %reduce-scatter.5.cloned.1.call-done = bf16[64,2048]{1,0:T(8,128)(2,1)} async-done(((bf16[128,2048]{1,0:T(8,128)(2,1)}), bf16[64,2048]{1,0:T(8,128)(2,1)}) %reduce-scatter.5.cloned.1.call-update) | async-done | bytes 262160 | tf_op jit(solution)/shard_map/reduce_scatter | solution.py:152
  449.6 1.7 add_convert_fusion
  (75 shorter events, 7.9 us)
Async XLA Ops:
  6.5 177.9 %copy-start = (bf16[512,2048]{1,0:T(8,128)(2,1)S(1)}, bf16[512,2048]{1,0:T(8,128)(2,1)}, u32[]{:S(2)}) copy-start(bf16[512,2048]{1,0:T(8,128)(2,1)} %param.26) | copy-start | bytes 6291460
  6.5 32.5 %copy-start.11 = (f32[128,8]{0,1:T(8,128)S(1)}, f32[128,8]{0,1:T(8,128)}, u32[]{:S(2)}) copy-start(f32[128,8]{0,1:T(8,128)} %param.24) | copy-start | bytes 12292
  6.5 57.6 %all-gather.11.cloned.1.call-start = ((), (), s32[]{:S(2)}) async-start(), calls=%async_computation.4 | async-start | bytes 2228224 | tf_op jit(solution)/shard_map/all_gather | solution.py:118
  7.3 94.8 %all-gather.9.cloned.1.call-start = ((), (), s32[]{:S(2)}) async-start(), calls=%async_computation.3 | async-start | bytes 2228224 | tf_op jit(solution)/shard_map/all_gather | solution.py:117
  9.0 144.7 %all-gather.7.cloned.1.call-start = ((), (), s32[]{:S(2)}) async-start(), calls=%async_computation.2 | async-start | bytes 4456448 | tf_op jit(solution)/shard_map/all_gather | solution.py:110
  10.8 189.8 %reduce-scatter.3.cloned.1.call-start = ((), (), s32[]{:S(2)}) async-start(), calls=%async_computation.5 | async-start | bytes 786432 | tf_op jit(solution)/shard_map/reduce_scatter | solution.py:124
  38.5 25.3 %copy-start.7 = (bf16[128,512]{1,0:T(8,128)(2,1)S(1)}, bf16[128,512]{1,0:T(8,128)(2,1)}, u32[]{:S(2)}) copy-start(bf16[128,512]{1,0:T(8,128)(2,1)} %param.18) | copy-start | bytes 393220
  63.3 38.7 %copy-start.12 = (bf16[128,512]{1,0:T(8,128)(2,1)S(1)}, bf16[128,512]{1,0:T(8,128)(2,1)}, u32[]{:S(2)}) copy-start(bf16[128,512]{1,0:T(8,128)(2,1)} %param.21) | copy-start | bytes 393220
  105.8 1.6 copy-start.6
  172.8 6.6 %copy-start.2 = (f32[8,2048,128]{2,1,0:T(8,128)S(1)}, f32[8,2048,128]{2,1,0:T(8,128)}, u32[]{:S(2)}) copy-start(f32[8,2048,128]{2,1,0:T(8,128)} %get-tuple-element.11) | copy-start | bytes 25165828
  184.4 1.6 copy-start.5
  184.4 4.8 %copy-start.8 = (f32[3,2048]{1,0:T(4,128)S(1)}, f32[3,2048]{1,0:T(4,128)}, u32[]{:S(2)}) copy-start(f32[3,2048]{1,0:T(4,128)} %param.31) | copy-start | bytes 73732
  184.4 4.8 %copy-start.9 = (f32[3,2048]{1,0:T(4,128)S(1)}, f32[3,2048]{1,0:T(4,128)}, u32[]{:S(2)}) copy-start(f32[3,2048]{1,0:T(4,128)} %param.32) | copy-start | bytes 73732
  184.4 16.2 %copy-start.3 = (bf16[64,2048]{1,0:T(8,128)(2,1)S(1)}, bf16[64,2048]{1,0:T(8,128)(2,1)}, u32[]{:S(2)}) copy-start(bf16[64,2048]{1,0:T(8,128)(2,1)} %param.17) | copy-start | bytes 786436
  184.5 17.3 %copy-start.10 = (f32[2048]{0:T(1024)S(1)}, f32[2048]{0:T(1024)}, u32[]{:S(2)}) copy-start(f32[2048]{0:T(1024)} %param.28) | copy-start | bytes 24580
  187.3 89.6 %all-gather.15.cloned.1.call-start = ((), (), s32[]{:S(2)}) async-start(), calls=%async_computation.7 | async-start | bytes 8912896 | tf_op jit(solution)/shard_map/all_gather | solution.py:86
  187.9 164.0 %all-gather.13.cloned.1.call-start = ((), (), s32[]{:S(2)}) async-start(), calls=%async_computation.6 | async-start | bytes 8912896 | tf_op jit(solution)/shard_map/all_gather | solution.py:85
  188.4 241.9 %all-gather.17.cloned.1.call-start = ((), (), s32[]{:S(2)}) async-start(), calls=%async_computation.8 | async-start | bytes 8912896 | tf_op jit(solution)/shard_map/all_gather | solution.py:87
  189.2 260.4 %reduce-scatter.5.cloned.1.call-start = ((), (), s32[]{:S(2)}) async-start(), calls=%async_computation.9 | async-start | bytes 786432 | tf_op jit(solution)/shard_map/reduce_scatter | solution.py:152
  356.5 3.0 collective-permute-start
  361.8 87.8 %copy-start.4 = (bf16[64,2048]{1,0:T(8,128)(2,1)S(1)}, bf16[64,2048]{1,0:T(8,128)(2,1)}, u32[]{:S(2)}) copy-start(bf16[64,2048]{1,0:T(8,128)(2,1)} %reduce-scatter.3.cloned.1.call-done) | copy-start | bytes 786436
  430.3 21.0 %copy-start.1 = (bf16[512,2048]{1,0:T(8,128)(2,1)S(1)}, bf16[512,2048]{1,0:T(8,128)(2,1)}, u32[]{:S(2)}) copy-start(bf16[512,2048]{1,0:T(8,128)(2,1)} %param.26) | copy-start | bytes 6291460
Sparse Core Ops, SparseCore 0:
  9.5 49.8 all-gather.10
  61.6 40.4 all-gather.8
  104.2 49.4 all-gather.6
  187.4 13.1 reduce-scatter.2
  202.6 74.2 all-gather.14
  278.9 72.8 all-gather.12
  354.0 76.2 all-gather.16
  436.8 12.7 reduce-scatter.4
